TPU v7x, 32 devices: a whole 2x2x4 slice. The times are simulated.
32 devices in a mesh: ep: 8 (over z, y), tp: 4 (over x, core).
Axes of the slice: x: 2, y: 2, z: 4, core: 2. Of those that a mesh axis runs over, the one named last changes fastest.
Arguments:
- tokens_first: bfloat16 [4096, 2048], P('ep'), may hold values from -6 to 6
- norm_gain_first: float32 [2048], replicated, may hold values from 0.1 to 1.9
- w_query: bfloat16 [2048, 512], P(None, 'tp'), may hold values from -0.125 to 0.125
- w_key: bfloat16 [2048, 512], P(None, 'tp'), may hold values from -0.125 to 0.125
- w_value: bfloat16 [2048, 1024], P(None, 'tp'), may hold values from -0.125 to 0.125
- w_outgate: bfloat16 [2048, 1024], P(None, 'tp'), may hold values from -0.125 to 0.125
- w_decay: bfloat16 [2048, 512], P(None, 'tp'), may hold values from -1 to 1
- decay_bias: float32 [64, 512], P('ep', 'tp'), may hold values from -1.3 to 12.5
- head_gain: float32 [1024], P('tp'), may hold values from 0.1 to 1.9
- w_mix_out: bfloat16 [1024, 2048], P('tp'), may hold values from -0.1875 to 0.1875
- tokens_second: bfloat16 [2048, 2048], P('ep'), may hold values from -6 to 6
- norm_gain_second: float32 [2048], replicated, may hold values from 0.1 to 1.9
- routes: int32 [2048, 2], P('ep'), may hold values from 0 to 7, all different within a row; in each aligned block of 256 rows (0 to 255, 256 to 511, ...) at most 128 rows name the same one
- route_logits: float32 [2048, 2], P('ep'), may hold values from -8 to 8
- expert_gate: bfloat16 [8, 2048, 3072], P('ep', None, 'tp'), may hold values from -0.125 to 0.125
- expert_up: bfloat16 [8, 2048, 3072], P('ep', None, 'tp'), may hold values from -0.125 to 0.125
- expert_down: bfloat16 [8, 3072, 2048], P('ep', 'tp'), may hold values from -0.109375 to 0.109375
Outputs:
- mixed_first: bfloat16 [4096, 2048], P(('ep', 'tp'))
- mixed_second: bfloat16 [2048, 2048], P('ep', 'tp')
Inputs may be any that keep to these rules, and one draw needn't show every extreme that they name: In the rows of one index of ep (aligned blocks of 256 rows) no expert is named by more than 128 rows, a bound that some block reaches; the two routes of a row name different experts.
All inputs are finite; a program needn't handle non-finite values.
Results may differ from a plain program's by a relative error of at most 0.01.
Values may be sent and summed in bfloat16 or wider, within the bound.
A program may use at most 128 MiB of HBM per device.

v0:
```python
import functools

import jax
import jax.numpy as jnp
from jax import lax
from jax.experimental import pallas as pl
from jax.experimental.pallas import tpu as pltpu
from jax.sharding import PartitionSpec as P

KEY_DIM = 64
VALUE_DIM = 128
BLOCK = 64
EPS = 1e-06
TEMPER = 16.0
CHUNKS = 4
LANES = 128

MESH = pl.DeviceIdType.MESH
F32 = jnp.float32
BF16 = jnp.bfloat16


def flip(index, mask):
    bit = 1
    while bit <= mask:
        if mask & bit:
            index = index + bit - 2 * bit * ((index // bit) % 2)
        bit *= 2
    return index


def dot(a, b):
    return jnp.dot(a, b, preferred_element_type=F32)


def dot_t(a, b, dims):
    return lax.dot_general(a, b, (dims, ((), ())), preferred_element_type=F32)


def rms_scale(wide):
    return lax.rsqrt(jnp.mean(wide * wide, axis=-1, keepdims=True) + EPS)


def kernel(
    n_ep,
    n_tp,
    tokens_first,
    gain_first,
    w_query,
    w_key,
    w_value,
    w_outgate,
    w_decay,
    decay_bias,
    head_gain,
    w_mix_out,
    tokens_second,
    gain_second,
    routes,
    routes_t,
    logits,
    e_gate,
    e_up,
    e_down,
    out_first,
    out_second,
    tf,
    wq,
    wk,
    wv,
    wg,
    wd,
    wm,
    ts,
    eg,
    eu,
    ed,
    normed,
    q_s,
    k_s,
    v_s,
    g_s,
    cum_s,
    state_s,
    st_send,
    fade_send,
    st_recv,
    fade_recv,
    inc,
    gated,
    mixp,
    mrecv1,
    msend,
    mrecv2,
    slots,
    rows,
    hid,
    part,
    recv1,
    send2,
    recv2,
    result,
    received,
    load_sem,
    disp_ss,
    disp_rs,
    xf_ss,
    xf_rs,
    cf_ss,
    cf_rs,
    st_ss,
    st_rs,
    fd_ss,
    fd_rs,
    m1_ss,
    m1_rs,
    m2_ss,
    m2_rs,
    r1_ss,
    r1_rs,
    r2_ss,
    r2_rs,
    ret_ss,
    ret_rs,
):
    e = lax.axis_index("ep")
    t = lax.axis_index("tp")
    lo = t % 2
    hi = t // 2
    near = flip(t, 1)
    far = flip(t, 2)
    cross = flip(t, 3)
    hi_other = 1 - hi

    loads = [
        pltpu.make_async_copy(src, dst, load_sem.at[i])
        for i, (src, dst) in enumerate(
            [
                (tokens_second, ts),
                (tokens_first, tf),
                (w_query, wq),
                (w_key, wk),
                (w_decay, wd),
                (w_value, wv),
                (w_outgate, wg),
                (e_gate, eg),
                (e_up, eu),
                (e_down, ed),
                (w_mix_out, wm),
            ]
        )
    ]
    for load in loads:
        load.start()

    barrier = pltpu.get_barrier_semaphore()
    for j in range(1, n_ep):
        pl.semaphore_signal(barrier, inc=1, device_id=(flip(e, j), t), device_id_type=MESH)
    for peer in (near, far):
        pl.semaphore_signal(barrier, inc=1, device_id=(e, peer), device_id_type=MESH)

    n_rows = ts.shape[0]
    n_slots, width = slots.shape
    room = n_slots // n_ep
    expert_col = lax.broadcasted_iota(jnp.int32, (LANES, n_rows), 0)
    rt = routes_t[...]
    m0 = (expert_col == rt[0:1, :]).astype(F32)
    m1 = (expert_col == rt[1:2, :]).astype(F32)
    r_i = lax.broadcasted_iota(jnp.int32, (n_rows, n_rows), 0)
    c_i = lax.broadcasted_iota(jnp.int32, (n_rows, n_rows), 1)
    before = dot((m0 + m1).astype(BF16), (r_i < c_i).astype(BF16))
    t0 = rt[0:1, :] * room + jnp.sum(m0 * before, axis=0, keepdims=True).astype(jnp.int32)
    t1 = rt[1:2, :] * room + jnp.sum(m1 * before, axis=0, keepdims=True).astype(jnp.int32)
    loads[0].wait()
    scale2 = rms_scale(ts[...].astype(F32))
    mine = pl.ds(pl.multiple_of(t * width, width), width)
    piece = (ts[:, mine].astype(F32) * scale2 * gain_second[:, mine]).astype(BF16)

    def build(i, carry):
        start = pl.multiple_of(i * 256, 256)
        slot_id = lax.broadcasted_iota(jnp.int32, (256, n_rows), 0) + start
        pick = ((slot_id == t0) | (slot_id == t1)).astype(F32).astype(BF16)
        slots[pl.ds(start, 256), :] = dot(pick, piece).astype(BF16)
        return carry

    lax.fori_loop(0, n_slots // 256, build, 0)

    def place(s):
        return pl.ds(pl.multiple_of(s * room, room), room)

    pl.semaphore_wait(barrier, n_ep + 1)

    def remote(src, dst, ss, rs, dev):
        return pltpu.make_async_remote_copy(
            src_ref=src, dst_ref=dst, send_sem=ss, recv_sem=rs, device_id=dev, device_id_type=MESH
        )

    disp = [None]
    for j in range(1, n_ep):
        s = flip(e, j)
        disp.append(
            remote(
                slots.at[place(s), :], rows.at[t, place(e), :], disp_ss.at[j], disp_rs.at[j], (s, t)
            )
        )
        disp[j].start()
    rows[t, place(e), :] = slots[place(e), :]

    xf, cf0, cf1 = [], [], []
    for j in range(n_ep):
        p = place(flip(e, j))
        xf.append(remote(rows.at[t, p, :], rows.at[t, p, :], xf_ss.at[j], xf_rs.at[j], (e, far)))
        cf0.append(
            remote(rows.at[t, p, :], rows.at[t, p, :], cf_ss.at[j, 0], cf_rs.at[j, 0], (e, near))
        )
        cf1.append(
            remote(
                rows.at[far, p, :], rows.at[far, p, :], cf_ss.at[j, 1], cf_rs.at[j, 1], (e, near)
            )
        )
    per_chunk = n_ep // CHUNKS

    def forward_own(c):
        for j in range(c * per_chunk, (c + 1) * per_chunk):
            if j > 0:
                disp[j].wait_recv()
            xf[j].start()
            cf0[j].start()

    def forward_far(c):
        for j in range(c * per_chunk, (c + 1) * per_chunk):
            xf[j].wait_recv()
            cf1[j].start()

    def arrived(c):
        for j in range(c * per_chunk, (c + 1) * per_chunk):
            cf0[j].wait_recv()
            cf1[j].wait_recv()

    xf[0].start()
    cf0[0].start()

    loads[1].wait()
    n_first = tf.shape[0]
    blocks = n_first // BLOCK

    def norm_rows(i, carry):
        at = pl.ds(pl.multiple_of(i * BLOCK, BLOCK), BLOCK)
        wide = tf[at, :].astype(F32)
        normed[at, :] = (wide * rms_scale(wide) * gain_first[...]).astype(BF16)
        return carry

    lax.fori_loop(0, blocks, norm_rows, 0)
    loads[2].wait()
    q_s[...] = (dot(normed[...], wq[...]) * KEY_DIM ** (-0.5)).astype(BF16)
    loads[3].wait()
    k_s[...] = dot(normed[...], wk[...]).astype(BF16)
    loads[4].wait()
    cum_s[...] = dot(normed[...], wd[...])
    for j in range(1, per_chunk):
        disp[j].wait_recv()
        xf[j].start()
        cf0[j].start()
    loads[5].wait()
    v_s[...] = dot(normed[...], wv[...]).astype(BF16)
    loads[6].wait()
    g_s[...] = dot(normed[...], wg[...])
    forward_own(1)
    forward_far(0)

    keys = k_s.shape[1]
    heads = keys // KEY_DIM
    tri_r = lax.broadcasted_iota(jnp.int32, (BLOCK, BLOCK), 0)
    tri_c = lax.broadcasted_iota(jnp.int32, (BLOCK, BLOCK), 1)
    causal = tri_r >= tri_c
    tri = causal.astype(F32)
    head_of = lax.broadcasted_iota(jnp.int32, (1, keys), 1) // KEY_DIM
    inc[...] = jnp.zeros_like(inc)

    def local_pass(b, total):
        at = pl.ds(pl.multiple_of(b * BLOCK, BLOCK), BLOCK)
        pre = cum_s[at, :] + decay_bias[pl.ds(b, 1), :]
        log_decay = (jnp.minimum(pre, 0.0) - jnp.log1p(jnp.exp(-jnp.abs(pre)))) / TEMPER
        cum = jnp.dot(tri, log_decay, precision=lax.Precision.HIGHEST, preferred_element_type=F32)
        cum_s[at, :] = cum
        last = cum[BLOCK - 1 : BLOCK, :]
        fading = (k_s[at, :].astype(F32) * jnp.exp(last - cum)).astype(BF16)
        full = dot_t(v_s[at, :], fading, ((0,), (0,)))
        add = full[0:VALUE_DIM]
        for h in range(1, heads):
            add = jnp.where(head_of == h, full[h * VALUE_DIM : (h + 1) * VALUE_DIM], add)
        state_s[b] = inc[...]
        inc[...] = inc[...] * jnp.exp(last) + add
        return total + last

    total = lax.fori_loop(0, blocks, local_pass, jnp.zeros((1, keys), F32))
    st_send[...] = inc[...].astype(BF16)
    fade_send[...] = jnp.broadcast_to(jnp.exp(total), fade_send.shape)

    def state_copies(k, dst):
        return (
            remote(st_send, st_recv.at[k], st_ss.at[k], st_rs.at[k], (dst, t)),
            remote(fade_send, fade_recv.at[k], fd_ss.at[k], fd_rs.at[k], (dst, t)),
        )

    for k in range(1, n_ep):

        @pl.when(e + k < n_ep)
        def _():
            for copy in state_copies(k, e + k):
                copy.start()

    chunk_rows = n_slots // CHUNKS
    hidden_width = hid.shape[1]
    tile = 256

    def chunk_at(c):
        m = flip(e // per_chunk, c)
        return pl.ds(pl.multiple_of(m * chunk_rows, chunk_rows), chunk_rows)

    def experts(c):
        at = chunk_at(c)

        def up(i, carry):
            cols = pl.ds(pl.multiple_of(i * tile, tile), tile)
            gate = jnp.zeros((chunk_rows, tile), F32)
            upper = jnp.zeros((chunk_rows, tile), F32)
            for b in range(n_tp):
                x = rows[b, at, :]
                gate = gate + dot(x, eg[0, b * width : (b + 1) * width, cols])
                upper = upper + dot(x, eu[0, b * width : (b + 1) * width, cols])
            hid[:, cols] = (gate * jax.nn.sigmoid(gate) * upper).astype(BF16)
            return carry

        lax.fori_loop(0, hidden_width // tile, up, 0)

        def down(b, carry):
            cols = pl.ds(pl.multiple_of(b * width, width), width)
            part[b, at, :] = dot(hid[...], ed[0, :, cols]).astype(BF16)
            return carry

        lax.fori_loop(0, n_tp, down, 0)

    near_lo = 1 - lo
    r1, r2, ret = [], [], []
    for c in range(CHUNKS):
        at = chunk_at(c)
        r1.append(
            [
                remote(
                    part.at[2 * h + near_lo, at, :],
                    recv1.at[h, at, :],
                    r1_ss.at[c, h],
                    r1_rs.at[c, h],
                    (e, near),
                )
                for h in range(2)
            ]
        )
        r2.append(remote(send2.at[at, :], recv2.at[at, :], r2_ss.at[c], r2_rs.at[c], (e, far)))
    for j in range(n_ep):
        s = flip(e, j)
        ret.append(
            remote(
                result.at[place(s), :], received.at[place(e), :], ret_ss.at[j], ret_rs.at[j], (s, t)
            )
        )

    def send_near(c):
        for copy in r1[c]:
            copy.start()

    def send_far(c):
        at = chunk_at(c)
        for copy in r1[c]:
            copy.wait_recv()
        send2[at, :] = (
            part[2 * hi_other + lo, at, :].astype(F32) + recv1[hi_other, at, :].astype(F32)
        ).astype(BF16)
        r2[c].start()

    def send_back(c):
        at = chunk_at(c)
        r2[c].wait_recv()
        result[at, :] = (
            part[t, at, :].astype(F32)
            + recv1[hi, at, :].astype(F32)
            + recv2[at, :].astype(F32)
        ).astype(BF16)
        for j in range(c * per_chunk, (c + 1) * per_chunk):
            if j > 0:
                ret[j].start()
        if c == 0:
            received[place(e), :] = result[place(e), :]

    forward_own(2)
    forward_far(1)
    for load in loads[7:10]:
        load.wait()
    arrived(0)
    experts(0)
    send_near(0)
    forward_own(3)
    forward_far(2)
    arrived(1)
    experts(1)
    send_near(1)
    send_far(0)
    forward_far(3)
    arrived(2)
    experts(2)
    send_near(2)
    send_far(1)
    send_back(0)
    arrived(3)
    experts(3)
    send_near(3)
    send_far(2)
    send_back(1)

    inc[...] = jnp.zeros_like(inc)
    for k in range(n_ep - 1, 0, -1):

        @pl.when(e >= k)
        def _():
            for copy in state_copies(k, e):
                copy.wait_recv()
            inc[...] = inc[...] * fade_recv[k, 0:1, :] + st_recv[k].astype(F32)

    def final_pass(b, before_log):
        at = pl.ds(pl.multiple_of(b * BLOCK, BLOCK), BLOCK)
        cum = cum_s[at, :]
        ahead = (q_s[at, :].astype(F32) * jnp.exp(cum)).astype(BF16)
        behind = (k_s[at, :].astype(F32) * jnp.exp(-cum)).astype(BF16)
        entry = (state_s[b] + inc[...] * jnp.exp(before_log)).astype(BF16)
        for h in range(heads):
            cols = slice(h * VALUE_DIM, (h + 1) * VALUE_DIM)
            own = jnp.where(head_of == h, ahead, jnp.zeros_like(ahead))
            scores = jnp.where(causal, dot_t(own, behind, ((1,), (1,))), 0.0)
            attended = dot(scores.astype(BF16), v_s[at, cols]) + dot_t(own, entry, ((1,), (1,)))
            gate = g_s[at, cols]
            gated[at, cols] = (
                attended
                * rms_scale(attended)
                * head_gain[:, cols]
                * (gate * jax.nn.sigmoid(gate))
            ).astype(BF16)
        return before_log + cum[BLOCK - 1 : BLOCK, :]

    lax.fori_loop(0, blocks, final_pass, jnp.zeros((1, keys), F32))
    loads[10].wait()
    mix_rows = n_first // n_tp

    def mix(i, carry):
        at = pl.ds(pl.multiple_of(i * mix_rows, mix_rows), mix_rows)
        mixp[i] = dot(gated[at, :], wm[...]).astype(BF16)
        return carry

    lax.fori_loop(0, n_tp, mix, 0)
    mix1 = [
        remote(
            mixp.at[2 * h + near_lo], mrecv1.at[h], m1_ss.at[h], m1_rs.at[h], (e, near)
        )
        for h in range(2)
    ]
    for copy in mix1:
        copy.start()
    send_far(3)
    send_back(2)
    for copy in mix1:
        copy.wait_recv()
    msend[...] = (
        mixp[2 * hi_other + lo].astype(F32) + mrecv1[hi_other].astype(F32)
    ).astype(BF16)
    mix2 = remote(msend, mrecv2, m2_ss.at[0], m2_rs.at[0], (e, far))
    mix2.start()
    send_back(3)
    mix2.wait_recv()
    out_first[...] = (
        mixp[t].astype(F32) + mrecv1[hi].astype(F32) + mrecv2[...].astype(F32)
    ).astype(BF16)

    col_expert = lax.broadcasted_iota(jnp.int32, (n_rows, LANES), 1)
    route = routes[...]
    n0 = (col_expert == route[:, 0:1]).astype(F32)
    n1 = (col_expert == route[:, 1:2]).astype(F32)
    ahead_of = dot((r_i > c_i).astype(BF16), (n0 + n1).astype(BF16))
    u0 = route[:, 0:1] * room + jnp.sum(n0 * ahead_of, axis=1, keepdims=True).astype(jnp.int32)
    u1 = route[:, 1:2] * room + jnp.sum(n1 * ahead_of, axis=1, keepdims=True).astype(jnp.int32)
    log0 = logits[:, 0:1]
    log1 = logits[:, 1:2]
    slot_col = lax.broadcasted_iota(jnp.int32, (n_rows, n_slots), 1)
    pick0 = (slot_col == u0).astype(F32).astype(BF16)
    pick1 = (slot_col == u1).astype(F32).astype(BF16)
    for j in range(1, n_ep):
        ret[j].wait_recv()
    out_second[...] = (
        dot(pick0, received[...]) * jax.nn.sigmoid(log0 - log1)
        + dot(pick1, received[...]) * jax.nn.sigmoid(log1 - log0)
    ).astype(BF16)

    for j in range(n_ep):
        if j > 0:
            disp[j].wait_send()
            ret[j].wait_send()
        xf[j].wait_send()
        cf0[j].wait_send()
        cf1[j].wait_send()
    for c in range(CHUNKS):
        for copy in r1[c]:
            copy.wait_send()
        r2[c].wait_send()
    for copy in mix1:
        copy.wait_send()
    mix2.wait_send()
    for k in range(1, n_ep):

        @pl.when(e + k < n_ep)
        def _():
            for copy in state_copies(k, e + k):
                copy.wait_send()


def body(
    tokens_first,
    norm_gain_first,
    w_query,
    w_key,
    w_value,
    w_outgate,
    w_decay,
    decay_bias,
    head_gain,
    w_mix_out,
    tokens_second,
    norm_gain_second,
    routes,
    route_logits,
    expert_gate,
    expert_up,
    expert_down,
):
    n_ep = lax.axis_size("ep")
    n_tp = lax.axis_size("tp")
    n_first, model = tokens_first.shape
    n_rows = tokens_second.shape[0]
    room = 2 * routes.shape[1] * n_rows // (n_ep * expert_gate.shape[0])
    n_slots = n_ep * room
    width = model // n_tp
    keys = w_query.shape[1]
    values = w_value.shape[1]
    hidden = expert_gate.shape[2]
    blocks = n_first // BLOCK
    mix_rows = n_first // n_tp
    chunk_rows = n_slots // CHUNKS
    vmem = pltpu.VMEM
    dma = pltpu.SemaphoreType.DMA

    def like(x):
        return vmem(x.shape, x.dtype)

    whole = pl.BlockSpec(memory_space=pltpu.VMEM)
    away = pl.BlockSpec(memory_space=pl.ANY)
    scratch = [
        like(tokens_first),
        like(w_query),
        like(w_key),
        like(w_value),
        like(w_outgate),
        like(w_decay),
        like(w_mix_out),
        like(tokens_second),
        like(expert_gate),
        like(expert_up),
        like(expert_down),
        vmem((n_first, model), BF16),
        vmem((n_first, keys), BF16),
        vmem((n_first, keys), BF16),
        vmem((n_first, values), BF16),
        vmem((n_first, values), F32),
        vmem((n_first, keys), F32),
        vmem((blocks, VALUE_DIM, keys), F32),
        vmem((VALUE_DIM, keys), BF16),
        vmem((8, keys), F32),
        vmem((n_ep, VALUE_DIM, keys), BF16),
        vmem((n_ep, 8, keys), F32),
        vmem((VALUE_DIM, keys), F32),
        vmem((n_first, values), BF16),
        vmem((n_tp, mix_rows, model), BF16),
        vmem((2, mix_rows, model), BF16),
        vmem((mix_rows, model), BF16),
        vmem((mix_rows, model), BF16),
        vmem((n_slots, width), BF16),
        vmem((n_tp, n_slots, width), BF16),
        vmem((chunk_rows, hidden), BF16),
        vmem((n_tp, n_slots, width), BF16),
        vmem((2, n_slots, width), BF16),
        vmem((n_slots, width), BF16),
        vmem((n_slots, width), BF16),
        vmem((n_slots, width), BF16),
        vmem((n_slots, width), BF16),
        dma((11,)),
        dma((n_ep,)),
        dma((n_ep,)),
        dma((n_ep,)),
        dma((n_ep,)),
        dma((n_ep, 2)),
        dma((n_ep, 2)),
        dma((n_ep,)),
        dma((n_ep,)),
        dma((n_ep,)),
        dma((n_ep,)),
        dma((2,)),
        dma((2,)),
        dma((1,)),
        dma((1,)),
        dma((CHUNKS, 2)),
        dma((CHUNKS, 2)),
        dma((CHUNKS,)),
        dma((CHUNKS,)),
        dma((n_ep,)),
        dma((n_ep,)),
    ]
    return pl.pallas_call(
        functools.partial(kernel, n_ep, n_tp),
        out_shape=(
            jax.ShapeDtypeStruct((mix_rows, model), BF16),
            jax.ShapeDtypeStruct((n_rows, width), BF16),
        ),
        in_specs=[away, whole, away, away, away, away, away, whole, whole, away]
        + [away, whole, whole, whole, whole, away, away, away],
        out_specs=(whole, whole),
        scratch_shapes=scratch,
        compiler_params=pltpu.CompilerParams(
            collective_id=0, has_side_effects=True, vmem_limit_bytes=60 * 1024 * 1024
        ),
    )(
        tokens_first,
        norm_gain_first[None, :],
        w_query,
        w_key,
        w_value,
        w_outgate,
        w_decay,
        decay_bias,
        head_gain[None, :],
        w_mix_out,
        tokens_second,
        norm_gain_second[None, :],
        routes,
        routes.T,
        route_logits,
        expert_gate,
        expert_up,
        expert_down,
    )


def solution(mesh):
    in_specs = (
        P("ep", None),
        P(),
        P(None, "tp"),
        P(None, "tp"),
        P(None, "tp"),
        P(None, "tp"),
        P(None, "tp"),
        P("ep", "tp"),
        P("tp"),
        P("tp", None),
        P("ep", None),
        P(),
        P("ep", None),
        P("ep", None),
        P("ep", None, "tp"),
        P("ep", None, "tp"),
        P("ep", "tp", None),
    )
    out_specs = (P(("ep", "tp"), None), P("ep", "tp"))
    return jax.shard_map(body, mesh=mesh, in_specs=in_specs, out_specs=out_specs, check_vma=False)
```

profile of v0, /device:TPU:8, one launch (start us, length us, event | category | flops | bytes accessed | tf_op | source)
XLA Modules:
  0.0 85.9 jit_solution(5395233321874005435)
XLA Ops:
  0.6 1.5 %copy.20.logits = f32[256,2]{1,0:T(8,128)} copy(f32[256,2]{0,1:T(2,128)} %param.30) | data formatting | bytes 4096 | tf_op args[13]
  2.1 1.5 %copy.19.routes = s32[256,2]{1,0:T(8,128)} copy(s32[256,2]{0,1:T(2,128)} %param.29) | data formatting | bytes 4096 | tf_op args[12]
  3.6 78.7 %shard_map.176 = (bf16[128,2048]{1,0:T(8,128)(2,1)}, bf16[256,512]{1,0:T(8,128)(2,1)}) custom-call(bf16[512,2048]{1,0:T(8,128)(2,1)} %tokens_first.1, f32[1,2048]{1,0:T(1,128)} %bitcast.4, bf16[2048,128]{1,0:T(8,128)(2,1)} %w_query.1, bf16[2048,128]{1,0:T(8,128)(2,1)} %w_key.1, bf16[2048,256]{1,0:T(8,128)(2,1)} %w_value.1, bf16[2048,256]{1,0:T(8,128)(2,1)} %w_outgate.1, ...), custom_call_target="tpu_custom_call" | custom-call | tf_op jit(solution)/shard_map/pallas_call | solution.py:624
  82.3 1.9 %copy.23 = bf16[128,2048]{1,0:T(8,128)(2,1)} copy(bf16[128,2048]{1,0:T(8,128)(2,1)} %get-tuple-element.4) | data formatting | bytes 1048576
  84.2 1.7 %copy.24 = bf16[256,512]{1,0:T(8,128)(2,1)} copy(bf16[256,512]{1,0:T(8,128)(2,1)} %get-tuple-element.5) | data formatting | bytes 524288
where the time goes:
time: 86.1 us; the launch traced here: 85.9 us
  Pallas kernels  78.7 us (91%)
  local copies, waits for them, and re-layouts  6.5 us (8%)
    pallas_call x1, Pallas kernels, body(): pl.pallas_call(functools.partial(kernel, n_ep, n_tp), out_shape=(jax.Shap...  78.7 us
    unnamed x4, local copies, waits for them, and re-layouts  6.5 us

commit v1 on v0

v1 whole, which is shorter than its diff:
```python
import functools

import jax
import jax.numpy as jnp
from jax import lax
from jax.experimental import pallas as pl
from jax.experimental.pallas import tpu as pltpu
from jax.sharding import PartitionSpec as P

KEY_DIM = 64
VALUE_DIM = 128
BLOCK = 64
EPS = 1e-06
TEMPER = 16.0
UNITS = 8
DIRECT = 4
DIRECT_OUT = 0
PIECES = 4
LANES = 128

MESH = pl.DeviceIdType.MESH
F32 = jnp.float32
BF16 = jnp.bfloat16


def flip(index, mask):
    bit = 1
    while bit <= mask:
        if mask & bit:
            index = index + bit - 2 * bit * ((index // bit) % 2)
        bit *= 2
    return index


def dot(a, b):
    return jnp.dot(a, b, preferred_element_type=F32)


def dot_t(a, b, dims):
    return lax.dot_general(a, b, (dims, ((), ())), preferred_element_type=F32)


def rms_scale(wide):
    return lax.rsqrt(jnp.mean(wide * wide, axis=-1, keepdims=True) + EPS)


def kernel(
    n_ep,
    n_tp,
    tokens_first,
    gain_first,
    w_query,
    w_key,
    w_value,
    w_outgate,
    w_decay,
    decay_bias,
    head_gain,
    w_mix_out,
    tokens_second,
    gain_second,
    routes_t,
    logits_t,
    e_gate,
    e_up,
    e_down,
    out_first,
    out_second,
    tf,
    wall,
    wm,
    ts,
    eg,
    eu,
    ed,
    normed2,
    normed,
    q_s,
    k_s,
    v_s,
    g_s,
    cum_s,
    state_s,
    st_send,
    fade_send,
    st_recv,
    fade_recv,
    half_send,
    half_recv,
    inc,
    gated,
    mixp,
    mrecv1,
    msend,
    mrecv2,
    slots,
    rows,
    hid,
    part,
    recv1,
    send2,
    recv2,
    result,
    received,
    result_d,
    received_d,
    info,
    keep,
    share_send,
    share_recv,
    load_sem,
    disp_ss,
    disp_rs,
    xf_ss,
    xf_rs,
    cf_ss,
    cf_rs,
    st_ss,
    st_rs,
    fd_ss,
    fd_rs,
    hf_ss,
    hf_rs,
    m1_ss,
    m1_rs,
    m2_ss,
    m2_rs,
    r1_ss,
    r1_rs,
    r2_ss,
    r2_rs,
    ret_ss,
    ret_rs,
    sh_ss,
    sh_rs,
):
    e = lax.axis_index("ep")
    t = lax.axis_index("tp")
    lo = t % 2
    hi = t // 2
    near = flip(t, 1)
    far = flip(t, 2)
    hi_other = 1 - hi
    near_lo = 1 - lo
    keys = k_s.shape[1]
    values = v_s.shape[1]

    loads = [
        pltpu.make_async_copy(src, dst, load_sem.at[i])
        for i, (src, dst) in enumerate(
            [
                (tokens_second, ts),
                (tokens_first, tf),
                (w_query, wall.at[:, 0:keys]),
                (w_key, wall.at[:, keys : 2 * keys]),
                (w_value, wall.at[:, 2 * keys : 2 * keys + values]),
                (w_outgate, wall.at[:, 2 * keys + values : 2 * keys + 2 * values]),
                (w_decay, wall.at[:, 2 * keys + 2 * values : 3 * keys + 2 * values]),
                (e_gate, eg),
                (e_up, eu),
                (e_down, ed),
                (w_mix_out, wm),
            ]
        )
    ]
    for load in loads:
        load.start()

    barrier = pltpu.get_barrier_semaphore()
    for j in range(1, n_ep):
        pl.semaphore_signal(barrier, inc=1, device_id=(flip(e, j), t), device_id_type=MESH)
    for peer in (near, far):
        pl.semaphore_signal(barrier, inc=1, device_id=(e, peer), device_id_type=MESH)

    n_rows = ts.shape[0]
    n_slots, width = received.shape
    room = n_slots // n_ep
    per = n_ep // UNITS
    unit_rows = n_slots // UNITS
    direct_slots = DIRECT * unit_rows

    def place(s):
        return pl.ds(pl.multiple_of(s * room, room), room)

    mine = e // per
    half = mine // 4
    inner = half + (mine // 2) % 2 == 1

    def unit(u):
        if u < 4:
            return flip(mine, u)
        mid = half if u < 6 else 1 - half
        return 4 * (1 - half) + 2 * mid + flip(mine % 2, u % 2)

    def chunk_at(u, n):
        m = unit(u) // n
        return pl.ds(pl.multiple_of(m * n * unit_rows, n * unit_rows), n * unit_rows)

    def members(u, n=1):
        return [
            (unit(v) * per + flip(e % per, k))
            for v in range(u, u + n)
            for k in range(per)
            if v > 0 or k > 0
        ]

    def cols_of(b):
        return pl.ds(pl.multiple_of(b * width, width), width)

    def remote(src, dst, ss, rs, dev):
        return pltpu.make_async_remote_copy(
            src_ref=src, dst_ref=dst, send_sem=ss, recv_sem=rs, device_id=dev, device_id_type=MESH
        )

    sends = []

    def launch(copy):
        copy.start()
        sends.append(copy)

    expert_col = lax.broadcasted_iota(jnp.int32, (LANES, n_rows), 0)
    rt = routes_t[...]
    m0 = (expert_col == rt[0:1, :]).astype(F32)
    m1 = (expert_col == rt[1:2, :]).astype(F32)
    r_i = lax.broadcasted_iota(jnp.int32, (n_rows, n_rows), 0)
    c_i = lax.broadcasted_iota(jnp.int32, (n_rows, n_rows), 1)
    before = dot((m0 + m1).astype(BF16), (r_i < c_i).astype(BF16))
    t0 = rt[0:1, :] * room + jnp.sum(m0 * before, axis=0, keepdims=True).astype(jnp.int32)
    t1 = rt[1:2, :] * room + jnp.sum(m1 * before, axis=0, keepdims=True).astype(jnp.int32)
    loads[0].wait()
    wide2 = ts[...].astype(F32)
    normed2[...] = (wide2 * rms_scale(wide2) * gain_second[...]).astype(BF16)

    def picks(start, count):
        slot_id = lax.broadcasted_iota(jnp.int32, (count, n_rows), 0) + start
        return ((slot_id == t0) | (slot_id == t1)).astype(F32).astype(BF16)

    tile = 256
    own_base = (e // (DIRECT * per)) * direct_slots

    def build_far(i, carry):
        start = pl.multiple_of((own_base + direct_slots + i * tile) % n_slots, tile)
        slots[0, pl.ds(start, tile), :] = dot(picks(start, tile), normed2[:, cols_of(t)]).astype(
            BF16
        )
        return carry

    def build_own(i, carry):
        start = pl.multiple_of(own_base + i * tile, tile)
        pick = picks(start, tile)
        for h, b in enumerate((t, far)):
            slots[h, pl.ds(start, tile), :] = dot(pick, normed2[:, cols_of(b)]).astype(BF16)
        return carry

    lax.fori_loop(0, (n_slots - direct_slots) // tile, build_far, 0)
    pl.semaphore_wait(barrier, n_ep + 1)

    def dispatch(s, h, sender):
        b = (t, far)[h]
        return remote(
            slots.at[h, place(s), :],
            rows.at[b, place(e), :],
            disp_ss.at[s, h],
            disp_rs.at[sender, h],
            (s, t),
        )

    straight = [dispatch(s, 0, e) for u in (4, 6) for s in members(u)]
    turning = [dispatch(s, 0, e) for u in (5, 7) for s in members(u)]
    sends.extend(straight + turning)

    @pl.when(inner)
    def _():
        for copy in straight:
            copy.start()

    lax.fori_loop(0, direct_slots // tile, build_own, 0)

    def dispatch_own(*units):
        for u in units:
            for s in members(u):
                for h in range(2):
                    launch(dispatch(s, h, e))

    def dispatch_turning():
        @pl.when(inner)
        def _():
            for copy in turning:
                copy.start()

    dispatch_own(1, 0, 2)

    def dispatch_outer():
        @pl.when(jnp.logical_not(inner))
        def _():
            for copy in straight + turning:
                copy.start()

    own_pick = picks(e * room, room)
    for b in range(n_tp):
        rows[b, place(e), :] = dot(own_pick, normed2[:, b * width : (b + 1) * width]).astype(BF16)

    def near_copy(s, h):
        at = rows.at[(t, far)[h], place(s), :]
        return remote(at, at, cf_ss.at[s, h], cf_rs.at[s, h], (e, near))

    def far_copy(s):
        at = rows.at[t, place(s), :]
        return remote(at, at, xf_ss.at[s], xf_rs.at[s], (e, far))

    def forward_own(u):
        for s in members(u):
            for h in range(2 if u < DIRECT else 1):
                dispatch(e, h, s).wait_recv()
            if u >= DIRECT:
                launch(far_copy(s))
            else:
                launch(near_copy(s, 1))
            launch(near_copy(s, 0))

    def forward_far(u):
        for s in members(u):
            far_copy(s).wait_recv()
            launch(near_copy(s, 1))

    def arrived(u):
        for s in members(u):
            for h in range(2):
                near_copy(s, h).wait_recv()

    n_first = tf.shape[0]
    blocks = n_first // BLOCK
    heads = keys // KEY_DIM
    tri_r = lax.broadcasted_iota(jnp.int32, (BLOCK, BLOCK), 0)
    tri_c = lax.broadcasted_iota(jnp.int32, (BLOCK, BLOCK), 1)
    causal = tri_r >= tri_c
    tri = causal.astype(F32)
    head_of = lax.broadcasted_iota(jnp.int32, (1, keys), 1) // KEY_DIM

    def norm_first():
        loads[1].wait()

        def norm_rows(i, carry):
            at = pl.ds(pl.multiple_of(i * BLOCK, BLOCK), BLOCK)
            wide = tf[at, :].astype(F32)
            normed[at, :] = (wide * rms_scale(wide) * gain_first[...]).astype(BF16)
            return carry

        lax.fori_loop(0, blocks, norm_rows, 0, unroll=2)

    def project():
        for load in loads[2:7]:
            load.wait()
        split = 2 * keys + values
        for start in range(0, n_first, tile):
            at = slice(start, start + tile)
            x = normed[at, :]
            left = dot(x, wall[:, 0:split])
            q_s[at, :] = (left[:, 0:keys] * KEY_DIM ** (-0.5)).astype(BF16)
            k_s[at, :] = left[:, keys : 2 * keys].astype(BF16)
            v_s[at, :] = left[:, 2 * keys : split].astype(BF16)
            right = dot(x, wall[:, split:])
            g_s[at, :] = right[:, 0:values]
            cum_s[at, :] = right[:, values:]

    group = n_ep // 2
    first_half = e < group
    spot = e % group

    def state_copies(k, sender):
        peer = e - spot + flip(spot, k)
        at = flip(spot, k) if sender else spot
        to = spot if sender else flip(spot, k)
        return (
            remote(st_send, st_recv.at[to], st_ss.at[at], st_rs.at[to], (peer, t)),
            remote(fade_send, fade_recv.at[to], fd_ss.at[at], fd_rs.at[to], (peer, t)),
        )

    def local_states():
        inc[...] = jnp.zeros_like(inc)

        def local_pass(b, total):
            at = pl.ds(pl.multiple_of(b * BLOCK, BLOCK), BLOCK)
            pre = cum_s[at, :] + decay_bias[pl.ds(b, 1), :]
            log_decay = (jnp.minimum(pre, 0.0) - jnp.log1p(jnp.exp(-jnp.abs(pre)))) / TEMPER
            cum = jnp.dot(
                tri, log_decay, precision=lax.Precision.HIGHEST, preferred_element_type=F32
            )
            cum_s[at, :] = cum
            last = cum[BLOCK - 1 : BLOCK, :]
            fading = (k_s[at, :].astype(F32) * jnp.exp(last - cum)).astype(BF16)
            full = dot_t(v_s[at, :], fading, ((0,), (0,)))
            add = full[0:VALUE_DIM]
            for h in range(1, heads):
                add = jnp.where(head_of == h, full[h * VALUE_DIM : (h + 1) * VALUE_DIM], add)
            state_s[b] = inc[...]
            inc[...] = inc[...] * jnp.exp(last) + add
            return total + last

        total = lax.fori_loop(0, blocks, local_pass, jnp.zeros((1, keys), F32), unroll=4)
        st_send[...] = inc[...].astype(BF16)
        fade_send[...] = jnp.broadcast_to(jnp.exp(total), fade_send.shape)
        st_recv[spot] = st_send[...]
        fade_recv[spot] = fade_send[...]
        for k in range(1, group):
            for copy in state_copies(k, True):
                launch(copy)

    half_copy = remote(half_send, half_recv, hf_ss.at[0], hf_rs.at[0], (flip(e, group), t))

    def fold(p):
        inc[...] = inc[...] * fade_recv[p, 0:1, :] + st_recv[p].astype(F32)

    def relay_state():
        for k in range(1, group):
            for copy in state_copies(k, False):
                copy.wait_recv()

        @pl.when(first_half)
        def _():
            inc[...] = jnp.zeros_like(inc)
            for p in range(group):
                fold(p)
            half_send[...] = inc[...].astype(BF16)
            half_copy.start()

    def share_table():
        lg = logits_t[...]
        row = lax.broadcasted_iota(jnp.int32, (LANES, n_rows), 0)
        parts = (
            t0.astype(F32),
            t1.astype(F32),
            jax.nn.sigmoid(lg[0:1, :] - lg[1:2, :]),
            jax.nn.sigmoid(lg[1:2, :] - lg[0:1, :]),
        )
        table = jnp.zeros((LANES, n_rows), F32)
        for i, line in enumerate(parts):
            table = jnp.where(row == i, line, table)
        info[...] = table.T

    def shares(u):
        start = unit(u) * unit_rows
        slot = lax.broadcasted_iota(jnp.int32, (n_rows, unit_rows), 1) + start
        slot = slot.astype(F32)
        return (
            jnp.where(slot == info[:, 0:1], info[:, 2:3], 0.0)
            + jnp.where(slot == info[:, 1:2], info[:, 3:4], 0.0)
        ).astype(BF16)

    hidden_width = hid.shape[1]

    def expert_weights():
        for load in loads[7:10]:
            load.wait()

    def experts(u, n):
        at = chunk_at(u, n)
        count = n * unit_rows

        for i in range(hidden_width // tile):
            cols = slice(i * tile, (i + 1) * tile)
            gate = jnp.zeros((count, tile), F32)
            upper = jnp.zeros((count, tile), F32)
            for b in range(n_tp):
                x = rows[b, at, :]
                gate = gate + dot(x, eg[0, b * width : (b + 1) * width, cols])
                upper = upper + dot(x, eu[0, b * width : (b + 1) * width, cols])
            hid[0:count, cols] = (gate * jax.nn.sigmoid(gate) * upper).astype(BF16)
        for b in range(n_tp):
            part[b, at, :] = dot(hid[0:count, :], ed[0, :, b * width : (b + 1) * width]).astype(
                BF16
            )

    r1, r2 = {}, {}

    def send_near(u, n):
        at = chunk_at(u, n)
        r1[u] = [
            remote(
                part.at[2 * h + near_lo, at, :],
                recv1.at[h, at, :],
                r1_ss.at[u, h],
                r1_rs.at[u, h],
                (e, near),
            )
            for h in range(2)
        ]
        for copy in r1[u]:
            launch(copy)

    def sum_far(u, n):
        at = chunk_at(u, n)
        for copy in r1[u]:
            copy.wait_recv()
        send2[at, :] = (
            part[2 * hi_other + lo, at, :].astype(F32) + recv1[hi_other, at, :].astype(F32)
        ).astype(BF16)

    def go_far(*units):
        for v in units:
            at = chunk_at(v, 1)
            r2[v] = remote(send2.at[at, :], recv2.at[at, :], r2_ss.at[v], r2_rs.at[v], (e, far))
            launch(r2[v])

    def send_far(u, n):
        sum_far(u, n)
        go_far(*range(u, u + n))

    def back_copy(s, sender):
        return remote(
            result.at[place(s), :],
            received.at[place(e), :],
            ret_ss.at[s, 0],
            ret_rs.at[sender, 0],
            (s, t),
        )

    def back_copy_d(s, h, sender):
        return remote(
            result_d.at[h, place(s), :],
            received_d.at[h, place(e), :],
            ret_ss.at[s, h],
            ret_rs.at[sender, h],
            (s, t),
        )

    def send_back(u, n):
        at = chunk_at(u, n)
        for v in range(u, u + n):
            r2[v].wait_recv()
        result[at, :] = (
            part[t, at, :].astype(F32)
            + recv1[hi, at, :].astype(F32)
            + recv2[at, :].astype(F32)
        ).astype(BF16)
        for s in members(u, n):
            launch(back_copy(s, e))
        if u == 0:
            received[place(e), :] = result[place(e), :]

    def send_direct(u, n):
        at = chunk_at(u, n)
        for copy in r1[u]:
            copy.wait_recv()
        for h in range(2):
            result_d[h, at, :] = (
                part[2 * h + lo, at, :].astype(F32) + recv1[h, at, :].astype(F32)
            ).astype(BF16)
        for s in members(u, n):
            for h in range(2):
                launch(back_copy_d(s, h, e))
        if u == 0:
            for h in range(2):
                received_d[h, place(e), :] = result_d[h, place(e), :]

    share_copy = remote(share_send, share_recv, sh_ss.at[0], sh_rs.at[0], (e, far))

    def combine_direct():
        for s in members(0, DIRECT_OUT):
            for h in range(2):
                back_copy_d(s, h, s).wait_recv()
        sums = [jnp.zeros((n_rows, width), F32) for _ in range(2)]
        for u in range(DIRECT_OUT):
            weights = shares(u)
            for i, h in enumerate((hi_other, hi)):
                sums[i] = sums[i] + dot(weights, received_d[h, chunk_at(u, 1), :])
        share_send[...] = sums[0].astype(BF16)
        launch(share_copy)
        keep[...] = sums[1]

    def gathered(u):
        for s in members(u):
            back_copy(s, s).wait_recv()
        return dot(shares(u), received[chunk_at(u, 1), :])

    def combine(*units):
        total = gathered(units[0])
        for u in units[1:]:
            total = total + gathered(u)
        if units[0] == 0:
            keep[...] = total
        else:
            keep[...] = keep[...] + total

    def combine_last(u):
        total = keep[...]
        if DIRECT_OUT:
            share_copy.wait_recv()
            total = total + share_recv[...].astype(F32)
        out_second[...] = (total + gathered(u)).astype(BF16)

    def attend():
        inc[...] = jnp.zeros_like(inc)

        @pl.when(jnp.logical_not(first_half))
        def _():
            half_copy.wait_recv()
            inc[...] = half_recv[...].astype(F32)

        for p in range(group - 1):

            @pl.when(spot > p)
            def _():
                fold(p)


        def final_pass(b, before_log):
            at = pl.ds(pl.multiple_of(b * BLOCK, BLOCK), BLOCK)
            cum = cum_s[at, :]
            ahead = (q_s[at, :].astype(F32) * jnp.exp(cum)).astype(BF16)
            behind = (k_s[at, :].astype(F32) * jnp.exp(-cum)).astype(BF16)
            entry = (state_s[b] + inc[...] * jnp.exp(before_log)).astype(BF16)
            for h in range(heads):
                cols = slice(h * VALUE_DIM, (h + 1) * VALUE_DIM)
                own = jnp.where(head_of == h, ahead, jnp.zeros_like(ahead))
                scores = jnp.where(causal, dot_t(own, behind, ((1,), (1,))), 0.0)
                attended = dot(scores.astype(BF16), v_s[at, cols]) + dot_t(
                    own, entry, ((1,), (1,))
                )
                gate = g_s[at, cols]
                gated[at, cols] = (
                    attended
                    * rms_scale(attended)
                    * head_gain[:, cols]
                    * (gate * jax.nn.sigmoid(gate))
                ).astype(BF16)
            return before_log + cum[BLOCK - 1 : BLOCK, :]

        lax.fori_loop(0, blocks, final_pass, jnp.zeros((1, keys), F32), unroll=4)

    mix_rows = n_first // n_tp
    mix1 = [
        remote(mixp.at[2 * h + near_lo], mrecv1.at[h], m1_ss.at[h], m1_rs.at[h], (e, near))
        for h in range(2)
    ]
    piece = mix_rows // PIECES

    def mix2(i):
        at = pl.ds(i * piece, piece)
        return remote(msend.at[at, :], mrecv2.at[at, :], m2_ss.at[i], m2_rs.at[i], (e, far))


    def mix_local():
        loads[10].wait()

        for i in range(n_tp):
            at = slice(i * mix_rows, (i + 1) * mix_rows)
            mixp[i] = dot(gated[at, :], wm[...]).astype(BF16)
        for copy in mix1:
            launch(copy)

    def mix_sum():
        for copy in mix1:
            copy.wait_recv()
        msend[...] = (
            mixp[2 * hi_other + lo].astype(F32) + mrecv1[hi_other].astype(F32)
        ).astype(BF16)

    def mix_far(*pieces):
        for i in pieces:
            launch(mix2(i))

    def mix_last():
        for i in range(PIECES):
            mix2(i).wait_recv()
        out_first[...] = (
            mixp[t].astype(F32) + mrecv1[hi].astype(F32) + mrecv2[...].astype(F32)
        ).astype(BF16)

    norm_first()
    project()
    dispatch_turning()
    dispatch_own(3)
    local_states()
    forward_own(4)
    expert_weights()
    share_table()
    experts(0, 1)
    send_near(0, 1)
    dispatch_outer()
    forward_far(4)
    send_far(0, 1)
    arrived(4)
    experts(4, 1)
    send_near(4, 1)
    forward_own(5)
    forward_own(1)
    forward_own(2)
    send_far(4, 1)
    arrived(2)
    experts(2, 1)
    send_near(2, 1)
    forward_far(5)
    arrived(1)
    experts(1, 1)
    send_near(1, 1)
    forward_own(3)
    arrived(5)
    experts(5, 1)
    send_near(5, 1)
    forward_own(6)
    send_back(4, 1)
    send_far(5, 1)
    send_far(1, 1)
    relay_state()
    arrived(3)
    experts(3, 1)
    send_near(3, 1)
    forward_far(6)
    forward_own(7)
    arrived(6)
    experts(6, 1)
    send_near(6, 1)
    send_far(2, 1)
    send_back(0, 1)
    send_back(5, 1)
    send_far(6, 1)
    attend()
    forward_far(7)
    arrived(7)
    experts(7, 1)
    send_near(7, 1)
    send_back(6, 1)
    send_back(1, 1)
    send_back(2, 1)
    send_far(7, 1)
    send_far(3, 1)
    mix_local()
    mix_sum()
    mix_far(0, 1, 2, 3)
    send_back(7, 1)
    send_back(3, 1)
    combine(0, 1, 2, 3)
    combine(4, 5, 6)
    mix_last()
    combine_last(7)
    for copy in sends:
        copy.wait_send()

    @pl.when(first_half)
    def _():
        half_copy.wait_send()


def hand_over(first, second, out_first, out_second, sems):
    copies = [
        pltpu.make_async_copy(first, out_first, sems.at[0]),
        pltpu.make_async_copy(second, out_second, sems.at[1]),
    ]
    for copy in copies:
        copy.start()
    for copy in copies:
        copy.wait()


def body(
    tokens_first,
    norm_gain_first,
    w_query,
    w_key,
    w_value,
    w_outgate,
    w_decay,
    decay_bias,
    head_gain,
    w_mix_out,
    tokens_second,
    norm_gain_second,
    routes,
    route_logits,
    expert_gate,
    expert_up,
    expert_down,
):
    n_ep = lax.axis_size("ep")
    n_tp = lax.axis_size("tp")
    n_first, model = tokens_first.shape
    n_rows = tokens_second.shape[0]
    room = 2 * routes.shape[1] * n_rows // (n_ep * expert_gate.shape[0])
    n_slots = n_ep * room
    width = model // n_tp
    keys = w_query.shape[1]
    values = w_value.shape[1]
    hidden = expert_gate.shape[2]
    blocks = n_first // BLOCK
    mix_rows = n_first // n_tp
    vmem = pltpu.VMEM
    dma = pltpu.SemaphoreType.DMA

    def like(x):
        return vmem(x.shape, x.dtype)

    whole = pl.BlockSpec(memory_space=pltpu.VMEM)
    away = pl.BlockSpec(memory_space=pl.ANY)
    scratch = [
        like(tokens_first),
        vmem((model, 3 * keys + 2 * values), BF16),
        like(w_mix_out),
        like(tokens_second),
        like(expert_gate),
        like(expert_up),
        like(expert_down),
        vmem((n_rows, model), BF16),
        vmem((n_first, model), BF16),
        vmem((n_first, keys), BF16),
        vmem((n_first, keys), BF16),
        vmem((n_first, values), BF16),
        vmem((n_first, values), F32),
        vmem((n_first, keys), F32),
        vmem((blocks, VALUE_DIM, keys), F32),
        vmem((VALUE_DIM, keys), BF16),
        vmem((8, keys), F32),
        vmem((n_ep // 2, VALUE_DIM, keys), BF16),
        vmem((n_ep // 2, 8, keys), F32),
        vmem((VALUE_DIM, keys), BF16),
        vmem((VALUE_DIM, keys), BF16),
        vmem((VALUE_DIM, keys), F32),
        vmem((n_first, values), BF16),
        vmem((n_tp, mix_rows, model), BF16),
        vmem((2, mix_rows, model), BF16),
        vmem((mix_rows, model), BF16),
        vmem((mix_rows, model), BF16),
        vmem((2, n_slots, width), BF16),
        vmem((n_tp, n_slots, width), BF16),
        vmem((n_slots // 4, hidden), BF16),
        vmem((n_tp, n_slots, width), BF16),
        vmem((2, n_slots, width), BF16),
        vmem((n_slots, width), BF16),
        vmem((n_slots, width), BF16),
        vmem((n_slots, width), BF16),
        vmem((n_slots, width), BF16),
        vmem((2, n_slots, width), BF16),
        vmem((2, n_slots, width), BF16),
        vmem((n_rows, LANES), F32),
        vmem((n_rows, width), F32),
        vmem((n_rows, width), BF16),
        vmem((n_rows, width), BF16),
        dma((11,)),
        dma((n_ep, 2)),
        dma((n_ep, 2)),
        dma((n_ep,)),
        dma((n_ep,)),
        dma((n_ep, 2)),
        dma((n_ep, 2)),
        dma((n_ep // 2,)),
        dma((n_ep // 2,)),
        dma((n_ep // 2,)),
        dma((n_ep // 2,)),
        dma((1,)),
        dma((1,)),
        dma((2,)),
        dma((2,)),
        dma((PIECES,)),
        dma((PIECES,)),
        dma((UNITS, 2)),
        dma((UNITS, 2)),
        dma((UNITS,)),
        dma((UNITS,)),
        dma((n_ep, 2)),
        dma((n_ep, 2)),
        dma((1,)),
        dma((1,)),
    ]
    first, second = pl.pallas_call(
        functools.partial(kernel, n_ep, n_tp),
        out_shape=(vmem((mix_rows, model), BF16), vmem((n_rows, width), BF16)),
        in_specs=[away, whole, away, away, away, away, away, whole, whole, away]
        + [away, whole, whole, whole, away, away, away],
        out_specs=(whole, whole),
        scratch_shapes=scratch,
        compiler_params=pltpu.CompilerParams(
            collective_id=0, has_side_effects=True, vmem_limit_bytes=60 * 1024 * 1024
        ),
    )(
        tokens_first,
        norm_gain_first[None, :],
        w_query,
        w_key,
        w_value,
        w_outgate,
        w_decay,
        decay_bias,
        head_gain[None, :],
        w_mix_out,
        tokens_second,
        norm_gain_second[None, :],
        routes.T,
        route_logits.T,
        expert_gate,
        expert_up,
        expert_down,
    )
    return pl.pallas_call(
        hand_over,
        out_shape=(
            jax.ShapeDtypeStruct((mix_rows, model), BF16),
            jax.ShapeDtypeStruct((n_rows, width), BF16),
        ),
        in_specs=[whole, whole],
        out_specs=(away, away),
        scratch_shapes=[dma((2,))],
    )(
        pltpu.with_memory_space_constraint(first, pltpu.VMEM),
        pltpu.with_memory_space_constraint(second, pltpu.VMEM),
    )


def solution(mesh):
    in_specs = (
        P("ep", None),
        P(),
        P(None, "tp"),
        P(None, "tp"),
        P(None, "tp"),
        P(None, "tp"),
        P(None, "tp"),
        P("ep", "tp"),
        P("tp"),
        P("tp", None),
        P("ep", None),
        P(),
        P("ep", None),
        P("ep", None),
        P("ep", None, "tp"),
        P("ep", None, "tp"),
        P("ep", "tp", None),
    )
    out_specs = (P(("ep", "tp"), None), P("ep", "tp"))
    return jax.shard_map(body, mesh=mesh, in_specs=in_specs, out_specs=out_specs, check_vma=False)
```

time: 86.1 us -> 73.2 us (0.85)
  the two profiles are of different devices: /device:TPU:8 before, /device:TPU:0 now
where the time goes in v1:
time: 73.2 us; the launch traced here: 73 us
  Pallas kernels  72.2 us (99%)
  between operations  0.81 us (1%)
    pallas_call x1, Pallas kernels, body(): pl.pallas_call(functools.partial(kernel, n_ep, n_tp), out_shape=(vmem((mi...  71.3 us

profile of v1, /device:TPU:0, one launch (start us, length us, event | category | flops | bytes accessed | tf_op | source)
XLA Modules:
  0.0 73.0 jit_solution(13480164155438891989)
XLA Ops:
  0.6 71.3 %shard_map.176 = (bf16[128,2048]{1,0:T(8,128)(2,1)S(1)}, bf16[256,512]{1,0:T(8,128)(2,1)S(1)}) custom-call(bf16[512,2048]{1,0:T(8,128)(2,1)} %tokens_first.1, f32[1,2048]{1,0:T(1,128)} %bitcast.5, bf16[2048,128]{1,0:T(8,128)(2,1)} %w_query.1, bf16[2048,128]{1,0:T(8,128)(2,1)} %w_key.1, bf16[2048,256]{1,0:T(8,128)(2,1)} %w_value.1, ...), custom_call_target="tpu_custom_call" | custom-call | tf_op jit(solution)/shard_map/pallas_call | solution.py:864
  71.9 0.9 %shard_map.177 = (bf16[128,2048]{1,0:T(8,128)(2,1)}, bf16[256,512]{1,0:T(8,128)(2,1)}) custom-call(bf16[128,2048]{1,0:T(8,128)(2,1)S(1)} %get-tuple-element.4.first, bf16[256,512]{1,0:T(8,128)(2,1)S(1)} %get-tuple-element.5.second), custom_call_target="tpu_custom_call" | custom-call | tf_op jit(solution)/shard_map/pallas_call | solution.py:893

commit v2 on v1

--- a/solution.py
+++ b/solution.py
@@ -14,8 +14,7 @@
 TEMPER = 16.0
 UNITS = 8
 DIRECT = 4
-DIRECT_OUT = 0
-PIECES = 4
+PIECES = 8
 LANES = 128
 
 MESH = pl.DeviceIdType.MESH
@@ -102,12 +101,8 @@
     recv2,
     result,
     received,
-    result_d,
-    received_d,
     info,
     keep,
-    share_send,
-    share_recv,
     load_sem,
     disp_ss,
     disp_rs,
@@ -131,8 +126,6 @@
     r2_rs,
     ret_ss,
     ret_rs,
-    sh_ss,
-    sh_rs,
 ):
     e = lax.axis_index("ep")
     t = lax.axis_index("tp")
@@ -306,7 +299,8 @@
 
     def far_copy(s):
         at = rows.at[t, place(s), :]
-        return remote(at, at, xf_ss.at[s], xf_rs.at[s], (e, far))
+        i = s % (n_ep // 2)
+        return remote(at, at, xf_ss.at[i], xf_rs.at[i], (e, far))
 
     def forward_own(u):
         for s in members(u):
@@ -467,7 +461,7 @@
                 upper = upper + dot(x, eu[0, b * width : (b + 1) * width, cols])
             hid[0:count, cols] = (gate * jax.nn.sigmoid(gate) * upper).astype(BF16)
         for b in range(n_tp):
-            part[b, at, :] = dot(hid[0:count, :], ed[0, :, b * width : (b + 1) * width]).astype(
+            part[b // 2, b % 2, at, :] = dot(hid[0:count, :], ed[0, :, b * width : (b + 1) * width]).astype(
                 BF16
             )
 
@@ -475,25 +469,16 @@
 
     def send_near(u, n):
         at = chunk_at(u, n)
-        r1[u] = [
-            remote(
-                part.at[2 * h + near_lo, at, :],
-                recv1.at[h, at, :],
-                r1_ss.at[u, h],
-                r1_rs.at[u, h],
-                (e, near),
-            )
-            for h in range(2)
-        ]
-        for copy in r1[u]:
-            launch(copy)
+        r1[u] = remote(
+            part.at[:, near_lo, at, :], recv1.at[:, at, :], r1_ss.at[u], r1_rs.at[u], (e, near)
+        )
+        launch(r1[u])
 
     def sum_far(u, n):
         at = chunk_at(u, n)
-        for copy in r1[u]:
-            copy.wait_recv()
+        r1[u].wait_recv()
         send2[at, :] = (
-            part[2 * hi_other + lo, at, :].astype(F32) + recv1[hi_other, at, :].astype(F32)
+            part[hi_other, lo, at, :].astype(F32) + recv1[hi_other, at, :].astype(F32)
         ).astype(BF16)
 
     def go_far(*units):
@@ -510,17 +495,8 @@
         return remote(
             result.at[place(s), :],
             received.at[place(e), :],
-            ret_ss.at[s, 0],
-            ret_rs.at[sender, 0],
-            (s, t),
-        )
-
-    def back_copy_d(s, h, sender):
-        return remote(
-            result_d.at[h, place(s), :],
-            received_d.at[h, place(e), :],
-            ret_ss.at[s, h],
-            ret_rs.at[sender, h],
+            ret_ss.at[s],
+            ret_rs.at[sender],
             (s, t),
         )
 
@@ -529,7 +505,7 @@
         for v in range(u, u + n):
             r2[v].wait_recv()
         result[at, :] = (
-            part[t, at, :].astype(F32)
+            part[hi, lo, at, :].astype(F32)
             + recv1[hi, at, :].astype(F32)
             + recv2[at, :].astype(F32)
         ).astype(BF16)
@@ -537,36 +513,6 @@
             launch(back_copy(s, e))
         if u == 0:
             received[place(e), :] = result[place(e), :]
-
-    def send_direct(u, n):
-        at = chunk_at(u, n)
-        for copy in r1[u]:
-            copy.wait_recv()
-        for h in range(2):
-            result_d[h, at, :] = (
-                part[2 * h + lo, at, :].astype(F32) + recv1[h, at, :].astype(F32)
-            ).astype(BF16)
-        for s in members(u, n):
-            for h in range(2):
-                launch(back_copy_d(s, h, e))
-        if u == 0:
-            for h in range(2):
-                received_d[h, place(e), :] = result_d[h, place(e), :]
-
-    share_copy = remote(share_send, share_recv, sh_ss.at[0], sh_rs.at[0], (e, far))
-
-    def combine_direct():
-        for s in members(0, DIRECT_OUT):
-            for h in range(2):
-                back_copy_d(s, h, s).wait_recv()
-        sums = [jnp.zeros((n_rows, width), F32) for _ in range(2)]
-        for u in range(DIRECT_OUT):
-            weights = shares(u)
-            for i, h in enumerate((hi_other, hi)):
-                sums[i] = sums[i] + dot(weights, received_d[h, chunk_at(u, 1), :])
-        share_send[...] = sums[0].astype(BF16)
-        launch(share_copy)
-        keep[...] = sums[1]
 
     def gathered(u):
         for s in members(u):
@@ -583,11 +529,7 @@
             keep[...] = keep[...] + total
 
     def combine_last(u):
-        total = keep[...]
-        if DIRECT_OUT:
-            share_copy.wait_recv()
-            total = total + share_recv[...].astype(F32)
-        out_second[...] = (total + gathered(u)).astype(BF16)
+        out_second[...] = (keep[...] + gathered(u)).astype(BF16)
 
     def attend():
         inc[...] = jnp.zeros_like(inc)
@@ -629,14 +571,11 @@
         lax.fori_loop(0, blocks, final_pass, jnp.zeros((1, keys), F32), unroll=4)
 
     mix_rows = n_first // n_tp
-    mix1 = [
-        remote(mixp.at[2 * h + near_lo], mrecv1.at[h], m1_ss.at[h], m1_rs.at[h], (e, near))
-        for h in range(2)
-    ]
+    mix1 = remote(mixp.at[:, near_lo], mrecv1, m1_ss.at[0], m1_rs.at[0], (e, near))
     piece = mix_rows // PIECES
 
     def mix2(i):
-        at = pl.ds(i * piece, piece)
+        at = pl.ds(0, piece) if i == 0 else pl.ds(piece, mix_rows - piece)
         return remote(msend.at[at, :], mrecv2.at[at, :], m2_ss.at[i], m2_rs.at[i], (e, far))
 
 
@@ -645,15 +584,13 @@
 
         for i in range(n_tp):
             at = slice(i * mix_rows, (i + 1) * mix_rows)
-            mixp[i] = dot(gated[at, :], wm[...]).astype(BF16)
-        for copy in mix1:
-            launch(copy)
+            mixp[i // 2, i % 2] = dot(gated[at, :], wm[...]).astype(BF16)
+        launch(mix1)
 
     def mix_sum():
-        for copy in mix1:
-            copy.wait_recv()
+        mix1.wait_recv()
         msend[...] = (
-            mixp[2 * hi_other + lo].astype(F32) + mrecv1[hi_other].astype(F32)
+            mixp[hi_other, lo].astype(F32) + mrecv1[hi_other].astype(F32)
         ).astype(BF16)
 
     def mix_far(*pieces):
@@ -661,17 +598,17 @@
             launch(mix2(i))
 
     def mix_last():
-        for i in range(PIECES):
+        for i in range(2):
             mix2(i).wait_recv()
         out_first[...] = (
-            mixp[t].astype(F32) + mrecv1[hi].astype(F32) + mrecv2[...].astype(F32)
+            mixp[hi, lo].astype(F32) + mrecv1[hi].astype(F32) + mrecv2[...].astype(F32)
         ).astype(BF16)
 
     norm_first()
     project()
     dispatch_turning()
+    local_states()
     dispatch_own(3)
-    local_states()
     forward_own(4)
     expert_weights()
     share_table()
@@ -684,56 +621,57 @@
     experts(4, 1)
     send_near(4, 1)
     forward_own(5)
-    forward_own(1)
     forward_own(2)
     send_far(4, 1)
     arrived(2)
     experts(2, 1)
     send_near(2, 1)
     forward_far(5)
+    relay_state()
+    forward_own(1)
+    send_far(2, 1)
+    arrived(5)
+    experts(5, 1)
+    send_near(5, 1)
+    send_back(4, 1)
     arrived(1)
     experts(1, 1)
     send_near(1, 1)
+    send_far(5, 1)
+    forward_own(6)
     forward_own(3)
-    arrived(5)
-    experts(5, 1)
-    send_near(5, 1)
-    forward_own(6)
-    send_back(4, 1)
-    send_far(5, 1)
     send_far(1, 1)
-    relay_state()
     arrived(3)
     experts(3, 1)
     send_near(3, 1)
     forward_far(6)
+    send_back(5, 1)
+    send_back(0, 1)
     forward_own(7)
+    send_far(3, 1)
     arrived(6)
     experts(6, 1)
     send_near(6, 1)
-    send_far(2, 1)
-    send_back(0, 1)
-    send_back(5, 1)
+    attend()
     send_far(6, 1)
-    attend()
+    mix_local()
+    send_back(2, 1)
     forward_far(7)
+    send_back(1, 1)
     arrived(7)
     experts(7, 1)
     send_near(7, 1)
+    mix_sum()
+    mix_far(0)
+    send_back(3, 1)
+    send_far(7, 1)
+    mix_far(1)
     send_back(6, 1)
-    send_back(1, 1)
-    send_back(2, 1)
-    send_far(7, 1)
-    send_far(3, 1)
-    mix_local()
-    mix_sum()
-    mix_far(0, 1, 2, 3)
     send_back(7, 1)
-    send_back(3, 1)
     combine(0, 1, 2, 3)
     combine(4, 5, 6)
+    combine_last(7)
     mix_last()
-    combine_last(7)
     for copy in sends:
         copy.wait_send()
 
@@ -816,30 +754,26 @@
         vmem((VALUE_DIM, keys), BF16),
         vmem((VALUE_DIM, keys), F32),
         vmem((n_first, values), BF16),
-        vmem((n_tp, mix_rows, model), BF16),
+        vmem((2, 2, mix_rows, model), BF16),
         vmem((2, mix_rows, model), BF16),
         vmem((mix_rows, model), BF16),
         vmem((mix_rows, model), BF16),
         vmem((2, n_slots, width), BF16),
         vmem((n_tp, n_slots, width), BF16),
         vmem((n_slots // 4, hidden), BF16),
-        vmem((n_tp, n_slots, width), BF16),
+        vmem((2, 2, n_slots, width), BF16),
         vmem((2, n_slots, width), BF16),
         vmem((n_slots, width), BF16),
         vmem((n_slots, width), BF16),
         vmem((n_slots, width), BF16),
         vmem((n_slots, width), BF16),
-        vmem((2, n_slots, width), BF16),
-        vmem((2, n_slots, width), BF16),
         vmem((n_rows, LANES), F32),
         vmem((n_rows, width), F32),
-        vmem((n_rows, width), BF16),
-        vmem((n_rows, width), BF16),
         dma((11,)),
         dma((n_ep, 2)),
         dma((n_ep, 2)),
-        dma((n_ep,)),
-        dma((n_ep,)),
+        dma((n_ep // 2,)),
+        dma((n_ep // 2,)),
         dma((n_ep, 2)),
         dma((n_ep, 2)),
         dma((n_ep // 2,)),
@@ -848,18 +782,16 @@
         dma((n_ep // 2,)),
         dma((1,)),
         dma((1,)),
+        dma((1,)),
+        dma((1,)),
         dma((2,)),
         dma((2,)),
-        dma((PIECES,)),
-        dma((PIECES,)),
-        dma((UNITS, 2)),
-        dma((UNITS, 2)),
         dma((UNITS,)),
         dma((UNITS,)),
-        dma((n_ep, 2)),
-        dma((n_ep, 2)),
-        dma((1,)),
-        dma((1,)),
+        dma((UNITS,)),
+        dma((UNITS,)),
+        dma((n_ep,)),
+        dma((n_ep,)),
     ]
     first, second = pl.pallas_call(
         functools.partial(kernel, n_ep, n_tp),

time: 73.2 us -> 67 us (0.915)
  Pallas kernels: 72.2 us -> 66 us
    pallas_call x1, Pallas kernels: 71.3 us -> 65.1 us  [body(): pl.pallas_call(functools.partial(kernel, n_ep, n_tp), out_shape=(vmem((mi...]
where the time goes in v2:
time: 67 us; the launch traced here: 66.8 us
  Pallas kernels  66 us (99%)
  between operations  0.81 us (1%)
    pallas_call x1, Pallas kernels, body(): pl.pallas_call(functools.partial(kernel, n_ep, n_tp), out_shape=(vmem((mi...  65.1 us

profile of v2, /device:TPU:0, one launch (start us, length us, event | category | flops | bytes accessed | tf_op | source)
XLA Modules:
  0.0 66.8 jit_solution(13584734239685671407)
XLA Ops:
  0.6 65.1 %shard_map.176 = (bf16[128,2048]{1,0:T(8,128)(2,1)S(1)}, bf16[256,512]{1,0:T(8,128)(2,1)S(1)}) custom-call(bf16[512,2048]{1,0:T(8,128)(2,1)} %tokens_first.1, f32[1,2048]{1,0:T(1,128)} %bitcast.5, bf16[2048,128]{1,0:T(8,128)(2,1)} %w_query.1, bf16[2048,128]{1,0:T(8,128)(2,1)} %w_key.1, bf16[2048,256]{1,0:T(8,128)(2,1)} %w_value.1, ...), custom_call_target="tpu_custom_call" | custom-call | tf_op jit(solution)/shard_map/pallas_call | solution.py:796
  65.7 0.9 %shard_map.177 = (bf16[128,2048]{1,0:T(8,128)(2,1)}, bf16[256,512]{1,0:T(8,128)(2,1)}) custom-call(bf16[128,2048]{1,0:T(8,128)(2,1)S(1)} %get-tuple-element.4.first, bf16[256,512]{1,0:T(8,128)(2,1)S(1)} %get-tuple-element.5.second), custom_call_target="tpu_custom_call" | custom-call | tf_op jit(solution)/shard_map/pallas_call | solution.py:825

commit v3 on v2

--- a/solution.py
+++ b/solution.py
@@ -637,35 +637,34 @@
     arrived(1)
     experts(1, 1)
     send_near(1, 1)
+    forward_own(6)
     send_far(5, 1)
-    forward_own(6)
     forward_own(3)
-    send_far(1, 1)
     arrived(3)
     experts(3, 1)
     send_near(3, 1)
     forward_far(6)
-    send_back(5, 1)
+    forward_own(7)
+    send_far(1, 1)
     send_back(0, 1)
-    forward_own(7)
-    send_far(3, 1)
     arrived(6)
     experts(6, 1)
     send_near(6, 1)
+    send_back(5, 1)
+    send_far(3, 1)
     attend()
     send_far(6, 1)
+    forward_far(7)
     mix_local()
     send_back(2, 1)
-    forward_far(7)
-    send_back(1, 1)
     arrived(7)
     experts(7, 1)
     send_near(7, 1)
+    send_back(1, 1)
     mix_sum()
-    mix_far(0)
+    send_far(7, 1)
+    mix_far(0, 1)
     send_back(3, 1)
-    send_far(7, 1)
-    mix_far(1)
     send_back(6, 1)
     send_back(7, 1)
     combine(0, 1, 2, 3)

time: 67 us -> 66.8 us (level)
  no operation moved by 1% of the time
where the time goes in v3:
time: 66.8 us; the launch traced here: 66.5 us
  Pallas kernels  65.7 us (98%)
  between operations  0.81 us (1%)
    pallas_call x1, Pallas kernels, body(): pl.pallas_call(functools.partial(kernel, n_ep, n_tp), out_shape=(vmem((mi...  64.8 us

profile of v3, /device:TPU:0, one launch (start us, length us, event | category | flops | bytes accessed | tf_op | source)
XLA Modules:
  0.0 66.5 jit_solution(10950145553308236193)
XLA Ops:
  0.6 64.8 %shard_map.176 = (bf16[128,2048]{1,0:T(8,128)(2,1)S(1)}, bf16[256,512]{1,0:T(8,128)(2,1)S(1)}) custom-call(bf16[512,2048]{1,0:T(8,128)(2,1)} %tokens_first.1, f32[1,2048]{1,0:T(1,128)} %bitcast.5, bf16[2048,128]{1,0:T(8,128)(2,1)} %w_query.1, bf16[2048,128]{1,0:T(8,128)(2,1)} %w_key.1, bf16[2048,256]{1,0:T(8,128)(2,1)} %w_value.1, ...), custom_call_target="tpu_custom_call" | custom-call | tf_op jit(solution)/shard_map/pallas_call | solution.py:795
  65.5 0.9 %shard_map.177 = (bf16[128,2048]{1,0:T(8,128)(2,1)}, bf16[256,512]{1,0:T(8,128)(2,1)}) custom-call(bf16[128,2048]{1,0:T(8,128)(2,1)S(1)} %get-tuple-element.4.first, bf16[256,512]{1,0:T(8,128)(2,1)S(1)} %get-tuple-element.5.second), custom_call_target="tpu_custom_call" | custom-call | tf_op jit(solution)/shard_map/pallas_call | solution.py:824
